TPU v7x, 32 devices: a whole 2x2x4 slice. The times are simulated.
32 devices in a mesh: grp: 2 (over y), sp: 4 (over z), tp: 4 (over x, core).
Axes of the slice: x: 2, y: 2, z: 4, core: 2. Of those that a mesh axis runs over, the one named last changes fastest.
Arguments:
- tokens: bfloat16 [3072, 2048], P(('grp', 'sp'), 'tp'), parts along dimension 0, may hold values from -6 to 6
- norm_gain: float32 [2048], replicated, may hold values from 0.1 to 1.9
- qk_gain: float32 [4, 64], replicated, may hold values from 0.7 to 5.5
- w_query_window: bfloat16 [2048, 1024], P('sp', 'tp'), may hold values from -1 to 1
- w_key_window: bfloat16 [2048, 512], P('sp', 'tp'), may hold values from -1 to 1
- w_value_window: bfloat16 [2048, 512], P('sp', 'tp'), may hold values from -0.125 to 0.125
- sink_logits: float32 [16], P('tp'), may hold values from 0 to 5
- w_query_forget: bfloat16 [2048, 1024], P('sp', 'tp'), may hold values from -1 to 1
- w_key_forget: bfloat16 [2048, 1024], P('sp', 'tp'), may hold values from -1 to 1
- w_value_forget: bfloat16 [2048, 1024], P('sp', 'tp'), may hold values from -0.125 to 0.125
- gate_cum: float32 [3072, 16], P(('grp', 'sp'), 'tp'), parts along dimension 0, as said below
- w_merge: bfloat16 [2048, 2, 2048], P('sp', None, 'tp'), may hold values from -0.125 to 0.125
- w_branch: bfloat16 [2, 1024, 2048], P(None, 'sp', 'tp'), may hold values from -0.8984375 to 0.8984375
Outputs:
- mixed: bfloat16 [3072, 2048], P(('grp', 'sp'), 'tp'), parts along dimension 0
There are 2 independent parts, one for each index of `grp`. A program takes and returns all parts, laid end to end along the dimension named above; an argument that names none is the same for every part. Nothing has to cross between parts.
Inputs may be any that keep to these rules, and one draw needn't show every extreme that they name: `gate_cum`: along positions each head's values never rise.
All inputs are finite; a program needn't handle non-finite values.
Results may differ from a plain program's by a relative error of at most 0.012.
Values may be sent and summed in bfloat16 or wider, within the bound.
A program may use at most 64 MiB of HBM per device.

v0:
```python
import math
import jax
import jax.numpy as jnp
from jax import lax
from jax.sharding import PartitionSpec as P

HEAD = 64
WINDOW = 128
epsilon = 1e-06
big_negative = -1e30


def from_behind(value, axis, by):
    size = lax.axis_size(axis)
    pairs = [(i, i + by) for i in range(size) if 0 <= i + by < size]
    return lax.ppermute(value, axis, pairs)


def head_norm(raw, gain, head_count):
    split = raw.reshape(raw.shape[0], head_count, -1)
    scaled = split * lax.rsqrt(jnp.mean(split * split, axis=-1, keepdims=True) + epsilon) * gain
    return scaled.astype(jnp.bfloat16)


def window_attend(queries, keys_ext, values_ext, sink_rows, first_pos):
    row_count, head_count, head_size = queries.shape
    group_count = keys_ext.shape[1]
    span_rows = WINDOW // 2
    block_count = row_count // span_rows
    query_blocks = queries.reshape(
        block_count, span_rows, group_count, head_count // group_count, head_size
    )
    key_blocks = jnp.concatenate(
        [
            keys_ext[lag_index * span_rows : lag_index * span_rows + row_count].reshape(
                block_count, span_rows, group_count, head_size
            )
            for lag_index in range(3)
        ],
        axis=1,
    )
    value_blocks = jnp.concatenate(
        [
            values_ext[lag_index * span_rows : lag_index * span_rows + row_count].reshape(
                block_count, span_rows, group_count, head_size
            )
            for lag_index in range(3)
        ],
        axis=1,
    )
    scores = jnp.einsum(
        "nqgrd,nkgd->ngrqk", query_blocks, key_blocks, preferred_element_type=jnp.float32
    ) * head_size ** (-0.5)
    distance = WINDOW + jnp.arange(span_rows)[:, None] - jnp.arange(3 * span_rows)[None, :]
    key_pos = (
        first_pos
        - WINDOW
        + jnp.arange(block_count)[:, None] * span_rows
        + jnp.arange(3 * span_rows)[None, :]
    )
    is_valid = ((distance >= 0) & (distance < WINDOW))[None] & (key_pos >= 0)[:, None, :]
    is_valid = is_valid[:, None, None]
    sink_grid = sink_rows.reshape(1, group_count, head_count // group_count, 1)
    row_max = jnp.maximum(jnp.max(jnp.where(is_valid, scores, big_negative), axis=-1), sink_grid)
    weights = jnp.where(is_valid, jnp.exp(scores - row_max[..., None]), 0.0)
    row_total = jnp.sum(weights, axis=-1) + jnp.exp(sink_grid - row_max)
    prob_rows = (weights / row_total[..., None]).astype(jnp.bfloat16)
    mixed_sum = jnp.einsum(
        "ngrqk,nkgd->nqgrd", prob_rows, value_blocks, preferred_element_type=jnp.float32
    )
    return mixed_sum.reshape(row_count, head_count * head_size).astype(jnp.bfloat16)


def forget_groups(groups, keys, values, gates):
    head_count, head_size = (keys.shape[1], keys.shape[2])
    gates_all = lax.all_gather(gates, "sp", axis=0, tiled=True)

    def absorber(queries, query_gate, query_pos):

        def absorb(running, block):
            row_max, row_total, mixed_sum = running
            key_rows, value_rows, key_gate, key_pos = block
            scores = jnp.einsum(
                "qhd,khd->hqk", queries, key_rows, preferred_element_type=jnp.float32
            ) * head_size ** (-0.5)
            scores = scores + query_gate.T[:, :, None] - key_gate.T[:, None, :]
            is_valid = (query_pos[:, None] >= key_pos[None, :])[None]
            new_max = jnp.maximum(
                row_max, jnp.max(jnp.where(is_valid, scores, big_negative), axis=-1)
            )
            weights = jnp.where(is_valid, jnp.exp(scores - new_max[..., None]), 0.0)
            shrink = jnp.exp(row_max - new_max)
            row_total = row_total * shrink + jnp.sum(weights, axis=-1)
            mixed_sum = mixed_sum * shrink.T[:, :, None] + jnp.einsum(
                "hqk,khd->qhd",
                weights.astype(jnp.bfloat16),
                value_rows,
                preferred_element_type=jnp.float32,
            )
            return ((new_max, row_total, mixed_sum), None)

        return absorb

    initial = tuple(
        (
            (
                jnp.full((head_count, group[0].shape[0]), big_negative, jnp.float32),
                jnp.zeros((head_count, group[0].shape[0]), jnp.float32),
                jnp.zeros((group[0].shape[0], head_count, head_size), jnp.float32),
            )
            for group in groups
        )
    )
    first_row = jnp.int32(0)
    key_rows = lax.all_gather(keys, "sp", axis=0, tiled=True)
    value_rows = lax.all_gather(values, "sp", axis=0, tiled=True)
    piece_rows = key_rows.shape[0]
    sub_rows = math.gcd(piece_rows, 2048)
    turns = piece_rows // sub_rows
    key_gate = gates_all
    key_pos = jnp.arange(piece_rows)
    blocks = (
        key_rows.reshape(turns, sub_rows, head_count, head_size),
        value_rows.reshape(turns, sub_rows, head_count, head_size),
        key_gate.reshape(turns, sub_rows, head_count),
        key_pos.reshape(turns, sub_rows),
    )
    updated = []
    for (queries, query_gate, query_pos), state in zip(groups, initial):
        absorb = absorber(queries, query_gate, query_pos)

        def advance(current):
            return lax.scan(absorb, current, blocks)[0]

        def keep(current):
            return current

        updated.append(lax.cond(first_row <= query_pos[-1], advance, keep, state))
    finals = tuple(updated)
    return [
        (mixed_sum / row_total.T[:, :, None])
        .reshape(mixed_sum.shape[0], head_count * head_size)
        .astype(jnp.bfloat16)
        for row_max, row_total, mixed_sum in finals
    ]


def on_device(
    tokens,
    norm_gain,
    qk_gain,
    w_query_window,
    w_key_window,
    w_value_window,
    sink_logits,
    w_query_forget,
    w_key_forget,
    w_value_forget,
    gate_cum,
    w_merge,
    w_branch,
):
    row_count = tokens.shape[0]
    row_offset = lax.axis_index("sp") * row_count
    gathered = lax.all_gather(tokens, "tp", axis=1, tiled=True)
    as_float = gathered.astype(jnp.float32)
    normed = (
        as_float
        * lax.rsqrt(jnp.mean(as_float * as_float, axis=-1, keepdims=True) + epsilon)
        * norm_gain
    ).astype(jnp.bfloat16)
    merge_flat = w_merge.reshape(w_merge.shape[0], -1)
    pieces = (
        lax.all_gather(w_query_window, "sp", axis=0, tiled=True),
        lax.all_gather(w_key_window, "sp", axis=0, tiled=True),
        lax.all_gather(w_value_window, "sp", axis=0, tiled=True),
        lax.all_gather(w_query_forget, "sp", axis=0, tiled=True),
        lax.all_gather(w_key_forget, "sp", axis=0, tiled=True),
        lax.all_gather(w_value_forget, "sp", axis=0, tiled=True),
        lax.all_gather(merge_flat, "sp", axis=0, tiled=True),
    )
    projected = tuple(
        (jnp.dot(normed, weight_rows, preferred_element_type=jnp.float32) for weight_rows in pieces)
    )
    query_heads = w_query_window.shape[1] // HEAD
    group_heads = w_key_window.shape[1] // HEAD
    window_query = head_norm(projected[0], qk_gain[0], query_heads)
    window_key = head_norm(projected[1], qk_gain[1], group_heads)
    window_value = projected[2].astype(jnp.bfloat16).reshape(row_count, group_heads, HEAD)
    prev_key, prev_value = from_behind(
        (window_key[row_count - WINDOW :], window_value[row_count - WINDOW :]), "sp", 1
    )
    window_out = window_attend(
        window_query,
        jnp.concatenate([prev_key, window_key], axis=0),
        jnp.concatenate([prev_value, window_value], axis=0),
        sink_logits,
        row_offset,
    )
    forget_query = head_norm(projected[3], qk_gain[2], query_heads)
    forget_key = head_norm(projected[4], qk_gain[3], query_heads)
    forget_value = projected[5].astype(jnp.bfloat16).reshape(row_count, query_heads, HEAD)
    own_pos = row_offset + jnp.arange(row_count)
    forget_out = forget_groups(
        [(forget_query, gate_cum, own_pos)], forget_key, forget_value, gate_cum
    )[0]
    channel_count = w_merge.shape[2]
    merge_gate = jax.nn.sigmoid(projected[6]).reshape(row_count, 2, channel_count)
    branch_full = lax.all_gather(w_branch, "sp", axis=1, tiled=True)
    head_stack = jnp.stack([window_out, forget_out], axis=1)
    weight_rows = branch_full
    projection = jnp.einsum(
        "uxa,xag->uxg",
        lax.all_gather(head_stack, "tp", axis=2, tiled=True),
        weight_rows,
        preferred_element_type=jnp.float32,
    )
    return (merge_gate[:, 0] * projection[:, 0] + merge_gate[:, 1] * projection[:, 1]).astype(
        jnp.bfloat16
    )


def solution(mesh):
    return jax.shard_map(
        on_device,
        mesh=mesh,
        in_specs=(
            P(("grp", "sp"), "tp"),
            P(),
            P(),
            P("sp", "tp"),
            P("sp", "tp"),
            P("sp", "tp"),
            P("tp"),
            P("sp", "tp"),
            P("sp", "tp"),
            P("sp", "tp"),
            P(("grp", "sp"), "tp"),
            P("sp", None, "tp"),
            P(None, "sp", "tp"),
        ),
        out_specs=P(("grp", "sp"), "tp"),
        check_vma=False,
    )
```

profile of v0, /device:TPU:0, one launch (start us, length us, event | category | flops | bytes accessed | tf_op | source)
XLA Modules:
  0.0 339.6 jit_solution(14842164746860835694)
XLA Ops:
  13.7 16.6 %all_gather.48 = f32[1536,4]{0,1:T(4,128)} all-gather(f32[384,4]{0,1:T(4,128)} %param.27), channel_id=1, replica_groups=mesh['grp'=2,'sp'=4,'tp'=4] {'sp'}, dimensions={0}, use_global_device_ids=true | all-gather | bytes 30720 | tf_op jit(solution)/shard_map/all_gather | solution.py:76
  30.5 19.0 %all_gather.42 = bf16[2048,128]{1,0:T(8,128)(2,1)} all-gather(bf16[512,128]{1,0:T(8,128)(2,1)S(1)} %copy-done.8), channel_id=1, replica_groups=mesh['grp'=2,'sp'=4,'tp'=4] {'sp'}, dimensions={0}, use_global_device_ids=true | all-gather | bytes 655360 | tf_op jit(solution)/shard_map/all_gather | solution.py:175
  50.2 21.1 %all_gather.41 = bf16[2048,128]{1,0:T(8,128)(2,1)} all-gather(bf16[512,128]{1,0:T(8,128)(2,1)S(1)} %copy-done.9), channel_id=1, replica_groups=mesh['grp'=2,'sp'=4,'tp'=4] {'sp'}, dimensions={0}, use_global_device_ids=true | all-gather | bytes 655360 | tf_op jit(solution)/shard_map/all_gather | solution.py:176
  74.3 2.5 multiply_reduce_fusion.1
  77.0 25.4 %all_gather.45 = bf16[1536,4,64]{0,2,1:T(8,128)(2,1)S(1)} all-gather(bf16[384,4,64]{0,2,1:T(8,128)(2,1)S(1)} %multiply_convert_fusion.2), channel_id=1, replica_groups=mesh['grp'=2,'sp'=4,'tp'=4] {'sp'}, dimensions={0}, use_global_device_ids=true | all-gather | bytes 983040 | tf_op jit(solution)/shard_map/all_gather | solution.py:115
  102.5 5.3 %all-gather.17.cloned.1.call-done = bf16[2048,256]{1,0:T(8,128)(2,1)} async-done(((bf16[512,256]{1,0:T(8,128)(2,1)}), bf16[2048,256]{1,0:T(8,128)(2,1)}) %all-gather.17.cloned.1.call-update) | async-done | bytes 1048592 | tf_op jit(solution)/shard_map/all_gather | solution.py:179
  109.7 25.2 %all_gather.47 = bf16[1536,4,64]{0,2,1:T(8,128)(2,1)S(1)} all-gather(bf16[384,4,64]{0,2,1:T(8,128)(2,1)S(1)} %bitcast.165), channel_id=1, replica_groups=mesh['grp'=2,'sp'=4,'tp'=4] {'sp'}, dimensions={0}, use_global_device_ids=true | all-gather | bytes 983040 | tf_op jit(solution)/shard_map/all_gather | solution.py:116
  134.9 8.7 %all-gather.19.cloned.1.call-done = bf16[2048,256]{1,0:T(8,128)(2,1)} async-done(((bf16[512,256]{1,0:T(8,128)(2,1)}), bf16[2048,256]{1,0:T(8,128)(2,1)}) %all-gather.19.cloned.1.call-update) | async-done | bytes 1048592 | tf_op jit(solution)/shard_map/all_gather | solution.py:177
  149.0 35.5 %conditional.1 = (f32[4,384]{1,0:T(4,128)}, f32[384,4,64]{0,2,1:T(8,128)}) conditional(s32[]{:T(128)} %bitcast.13, () %tuple.20, (bf16[1536,4,64]{0,2,1:T(8,128)(2,1)S(1)}, bf16[1536,4,64]{0,2,1:T(8,128)(2,1)S(1)}, f32[1536,4]{0,1:T(4,128)}, s32[3,512]{1,0:T(4,128)S(1)}, s32[3,512]{1,0:T(4,128)S(1)}, /*index=5*/s32[384]{0:T(512)}, ...), branch_computations={%region_7.8_spmd, %region_8.13_spmd} | conditional | flops 215199744 | bytes 15060769 | solution.py:138
  151.0 33.5 %while.18 = (s32[]{:T(128)}, f32[4,384]{1,0:T(4,128)S(1)}, f32[4,384]{1,0:T(4,128)}, f32[384,4,64]{0,2,1:T(8,128)}, s32[384]{0:T(512)}, /*index=5*/s32[3,512]{1,...) while((s32[]{:T(128)}, f32[4,384]{1,0:T(4,128)S(1)}, ...), condition=%wide.region_12.12_spmd.clone, body=%wide.region_9.11_spmd.clone.sunk | while | flops 215196672 | bytes 11896481 | solution.py:133
  153.2 2.7 fusion.85
  158.8 2.7 fusion.89
  163.8 2.7 fusion.85
  170.1 2.9 fusion.89
  175.3 2.7 fusion.85
  181.6 2.9 fusion.89
  189.8 2.8 collective-permute-start.1
  192.6 3.3 collective-permute-start
  203.8 14.9 %all-gather.23.cloned.1.call-done = bf16[2,1024,512]{2,1,0:T(8,128)(2,1)} async-done(((bf16[2,256,512]{2,1,0:T(8,128)(2,1)}), bf16[2,1024,512]{2,1,0:T(8,128)(2,1)}) %all-gather.23.cloned.1.call-update) | async-done | bytes 2097168 | tf_op jit(solution)/shard_map/all_gather | solution.py:209
  218.6 21.5 %all-gather.21.cloned.1.call-done = bf16[384,2,1024]{2,0,1:T(8,128)(2,1)} async-done(((bf16[384,2,256]{2,0,1:T(8,128)(2,1)}), bf16[384,2,1024]{2,0,1:T(8,128)(2,1)}) %all-gather.21.cloned.1.call-update) | async-done | bytes 1572880 | tf_op jit(solution)/shard_map/all_gather | solution.py:214
  240.2 3.0 convolution_bitcast_fusion
  243.2 79.3 %all-gather.11.cloned.1.call-done = bf16[2048,1024]{1,0:T(8,128)(2,1)} async-done(((bf16[512,1024]{1,0:T(8,128)(2,1)}), bf16[2048,1024]{1,0:T(8,128)(2,1)}) %all-gather.11.cloned.1.call-update) | async-done | bytes 4194320 | tf_op jit(solution)/shard_map/all_gather | solution.py:180
  322.5 5.3 %add_divide_fusion = f32[384,1024]{1,0:T(8,128)} fusion(bf16[384,2048]{1,0:T(8,128)(2,1)S(1)} %copy-done.1, bf16[2048,1024]{1,0:T(8,128)(2,1)} %all-gather.11.cloned.1.call-done), kind=kOutput, calls=%fused_computation.44 | convolution fusion | flops 1611792384 | bytes 7340032 | tf_op jit(solution)/shard_map/dot_general | solution.py:183
  327.8 2.6 reshape.258
  (143 shorter events, 51.7 us)
Async XLA Ops:
  6.5 6.6 %copy-start.15 = (f32[4,64]{1,0:T(4,128)S(1)}, f32[4,64]{1,0:T(4,128)}, u32[]{:S(2)}) copy-start(f32[4,64]{1,0:T(4,128)} %param.19) | copy-start | bytes 3076
  6.5 24.0 %copy-start.8 = (bf16[512,128]{1,0:T(8,128)(2,1)S(1)}, bf16[512,128]{1,0:T(8,128)(2,1)}, u32[]{:S(2)}) copy-start(bf16[512,128]{1,0:T(8,128)(2,1)} %param.21) | copy-start | bytes 393220
  6.5 42.9 %copy-start.16 = (f32[4]{0:T(128)S(1)}, f32[4]{0:T(128)}, u32[]{:S(2)}) copy-start(f32[4]{0:T(128)} %param.23) | copy-start | bytes 52
  6.5 43.6 %copy-start.9 = (bf16[512,128]{1,0:T(8,128)(2,1)S(1)}, bf16[512,128]{1,0:T(8,128)(2,1)}, u32[]{:S(2)}) copy-start(bf16[512,128]{1,0:T(8,128)(2,1)} %param.22) | copy-start | bytes 393220
  6.5 65.4 %all-gather.9.cloned.1.call-start = ((), (), s32[]{:S(2)}) async-start(), calls=%async_computation | async-start | bytes 1966080 | tf_op jit(solution)/shard_map/all_gather | solution.py:165
  7.3 67.1 %all-gather.15.cloned.1.call-start = ((), (), s32[]{:S(2)}) async-start(), calls=%async_computation.3 | async-start | bytes 1310720 | tf_op jit(solution)/shard_map/all_gather | solution.py:178
  8.0 99.7 %all-gather.17.cloned.1.call-start = ((), (), s32[]{:S(2)}) async-start(), calls=%async_computation.4 | async-start | bytes 1310720 | tf_op jit(solution)/shard_map/all_gather | solution.py:179
  8.8 134.9 %all-gather.19.cloned.1.call-start = ((), (), s32[]{:S(2)}) async-start(), calls=%async_computation.5 | async-start | bytes 1310720 | tf_op jit(solution)/shard_map/all_gather | solution.py:177
  9.3 176.2 %all-gather.13.cloned.1.call-start = ((), (), s32[]{:S(2)}) async-start(), calls=%async_computation.2 | async-start | bytes 1310720 | tf_op jit(solution)/shard_map/all_gather | solution.py:174
  9.9 208.7 %all-gather.23.cloned.1.call-start = ((), (), s32[]{:S(2)}) async-start(), calls=%async_computation.7 | async-start | bytes 2621440 | tf_op jit(solution)/shard_map/all_gather | solution.py:209
  10.5 63.4 %copy-start.11 = (f32[2048]{0:T(1024)S(1)}, f32[2048]{0:T(1024)}, u32[]{:S(2)}) copy-start(f32[2048]{0:T(1024)} %param.18) | copy-start | bytes 24580
  10.5 229.6 %all-gather.21.cloned.1.call-start = ((), (), s32[]{:S(2)}) async-start(), calls=%async_computation.6 | async-start | bytes 1966080 | tf_op jit(solution)/shard_map/all_gather | solution.py:214
  71.9 1.9 copy-start.2
  74.3 72.6 %copy-start = (bf16[384,2048]{1,0:T(8,128)(2,1)}, bf16[384,2048]{1,0:T(8,128)(2,1)S(1)}, u32[]{:S(2)}) copy-start(bf16[384,2048]{1,0:T(8,128)(2,1)S(1)} %fusion.27) | copy-start | bytes 4718596
  143.7 2.1 copy-start.3
  145.7 1.2 copy-start.4
  185.5 2.6 copy-start.5
  188.4 1.2 copy-start.12
  188.6 7.3 %copy-start.14 = (f32[64]{0:T(128)S(1)}, f32[64]{0:T(128)}, u32[]{:S(2)}) copy-start(f32[64]{0:T(128)} %get-tuple-element.195) | copy-start | bytes 772
  189.8 7.2 %collective-permute-start.1 = (bf16[128,2,64]{0,2,1:T(8,128)(2,1)S(1)}, bf16[128,2,64]{0,2,1:T(8,128)(2,1)S(1)}, u32[]{:S(2)}, u32[]{:S(2)}) collective-permute-start(bf16[128,2,64]{0,2,1:T(8,128)(2,1)S(1)} %slice.68), channel_id=1, source_target_pairs={{0,4},{4,8},{8,12},{1,5},{5,9},{9,13},{2,6},{6,10},{10,14},{3,7},{... | collective-permute-start | bytes 98312 | tf_op jit(solution)/shard_map/ppermute | solution.py:16
  192.6 5.4 %collective-permute-start = (bf16[128,2,64]{0,2,1:T(8,128)(2,1)S(1)}, bf16[128,2,64]{0,2,1:T(8,128)(2,1)S(1)}, u32[]{:S(2)}, u32[]{:S(2)}) collective-permute-start(bf16[128,2,64]{0,2,1:T(8,128)(2,1)S(1)} %bitcast.167), channel_id=1, source_target_pairs={{0,4},{4,8},{8,12},{1,5},{5,9},{9,13},{2,6},{6,10},{10,14},{3,7},{... | collective-permute-start | bytes 98312 | tf_op jit(solution)/shard_map/ppermute | solution.py:16
  200.9 1.5 copy-start.6
  202.4 120.1 %all-gather.11.cloned.1.call-start = ((), (), s32[]{:S(2)}) async-start(), calls=%async_computation.1 | async-start | bytes 5242880 | tf_op jit(solution)/shard_map/all_gather | solution.py:180
  203.8 118.7 %copy-start.1 = (bf16[384,2048]{1,0:T(8,128)(2,1)S(1)}, bf16[384,2048]{1,0:T(8,128)(2,1)}, u32[]{:S(2)}) copy-start(bf16[384,2048]{1,0:T(8,128)(2,1)} %copy-done) | copy-start | bytes 4718596
  (3 other events, 3.0 us)
Sparse Core Ops, SparseCore 0:
  8.9 22.3 all-gather.8
  32.9 36.9 all-gather.14
  71.5 36.1 all-gather.16
  109.1 34.4 all-gather.18
  145.1 27.0 all-gather.12
  173.6 45.0 all-gather.22
  220.2 19.9 all-gather.20
  241.7 80.7 all-gather.10
where the time goes:
time: 341 us; the launch traced here: 340 us
  waiting for transfers between devices  134 us (39%)
  blocking collectives  107 us (31%)
  matrix products  37.9 us (11%)
  other arithmetic  23.1 us (7%)
  local copies, waits for them, and re-layouts  16.3 us (5%)
  between operations  14.7 us (4%)
  starting transfers between devices  6.38 us (2%)
    all_gather x1, waiting for transfers between devices, on_device(): lax.all_gather(merge_flat, 'sp', axis=0, tiled=True)  79.3 us
    all_gather x1, blocking collectives, forget_groups(): key_rows = lax.all_gather(keys, 'sp', axis=0, tiled=True)  25.4 us
    all_gather x1, blocking collectives, forget_groups(): value_rows = lax.all_gather(values, 'sp', axis=0, tiled=True)  25.2 us
    all_gather x1, waiting for transfers between devices, on_device(): lax.all_gather(head_stack, 'tp', axis=2, tiled=True)  21.5 us
    all_gather x1, blocking collectives, on_device(): lax.all_gather(w_value_window, 'sp', axis=0, tiled=True)  21.1 us
    all_gather x1, blocking collectives, on_device(): lax.all_gather(w_key_window, 'sp', axis=0, tiled=True)  19 us
    dot_general x7, matrix products, on_device(): jnp.dot(normed, weight_rows, preferred_element_type=jnp.float32)  16.8 us
    all_gather x1, blocking collectives, forget_groups(): gates_all = lax.all_gather(gates, 'sp', axis=0, tiled=True)  16.6 us
  transfers between devices with their start and end apart: 10, of which 6 were waited for; matrix products, arithmetic and copies ran while one was open for 20% of the time, Pallas kernels for 0%

commit v1 on v0

--- a/solution.py
+++ b/solution.py
@@ -113,7 +113,12 @@
     )
     first_row = jnp.int32(0)
     key_rows = lax.all_gather(keys, "sp", axis=0, tiled=True)
-    value_rows = lax.all_gather(values, "sp", axis=0, tiled=True)
+    ring = [values]
+    for hop in range(3):
+        ring.append(lax.ppermute(ring[-1], "sp", [(dev, (dev + 1) % 4) for dev in range(4)]))
+    value_rows = jnp.roll(
+        jnp.concatenate(ring[::-1], axis=0), (lax.axis_index("sp") + 1) * ring[0].shape[0], axis=0
+    )
     piece_rows = key_rows.shape[0]
     sub_rows = math.gcd(piece_rows, 2048)
     turns = piece_rows // sub_rows

time: 341 us -> 370 us (1.085)
  waiting for transfers between devices: 134 us -> 169 us
  blocking collectives: 107 us -> 82.5 us
  local copies, waits for them, and re-layouts: 16.3 us -> 25.8 us
  starting transfers between devices: 6.38 us -> 10.7 us
    all_gather x1, waiting for transfers between devices: 0.02 us -> 25.7 us  [on_device(): lax.all_gather(w_query_window, 'sp', axis=0, tiled=True)]
    all_gather x1 -> x0, blocking collectives: 25.2 us -> none  [forget_groups(): value_rows = lax.all_gather(values, 'sp', axis=0, tiled=True)]
    ppermute x0 -> x3, waiting for transfers between devices: none -> 24.3 us  [forget_groups(): lax.ppermute(ring[-1], 'sp', [(dev, (dev + 1) % 4) for dev in range(4)])]
    all_gather x1, waiting for transfers between devices: 14.9 us -> 0.02 us  [on_device(): branch_full = lax.all_gather(w_branch, 'sp', axis=1, tiled=True)]
  transfers between devices with their start and end apart: 10 -> 13, of which waited for: 6 -> 7; matrix products, arithmetic and copies ran while one was open for 20% -> 22% of each run, Pallas kernels for 0% -> 0%
where the time goes in v1:
time: 370 us; the launch traced here: 368 us
  waiting for transfers between devices  169 us (46%)
  blocking collectives  82.5 us (22%)
  matrix products  39.1 us (11%)
  other arithmetic  26.1 us (7%)
  local copies, waits for them, and re-layouts  25.8 us (7%)
  between operations  14.7 us (4%)
  starting transfers between devices  10.7 us (3%)
    all_gather x1, waiting for transfers between devices, on_device(): lax.all_gather(merge_flat, 'sp', axis=0, tiled=True)  79.3 us
    all_gather x1, waiting for transfers between devices, on_device(): lax.all_gather(w_query_window, 'sp', axis=0, tiled=True)  25.7 us
    all_gather x1, blocking collectives, forget_groups(): key_rows = lax.all_gather(keys, 'sp', axis=0, tiled=True)  25.7 us
    ppermute x3, waiting for transfers between devices, forget_groups(): lax.ppermute(ring[-1], 'sp', [(dev, (dev + 1) % 4) for dev in range(4)])  24.3 us
    all_gather x1, waiting for transfers between devices, on_device(): lax.all_gather(head_stack, 'tp', axis=2, tiled=True)  22.5 us
    all_gather x1, blocking collectives, on_device(): lax.all_gather(w_value_window, 'sp', axis=0, tiled=True)  22 us
    all_gather x1, blocking collectives, on_device(): lax.all_gather(w_key_window, 'sp', axis=0, tiled=True)  18.2 us
    dot_general x7, matrix products, on_device(): jnp.dot(normed, weight_rows, preferred_element_type=jnp.float32)  17.1 us
  transfers between devices with their start and end apart: 13, of which 7 were waited for; matrix products, arithmetic and copies ran while one was open for 22% of the time, Pallas kernels for 0%

profile of v1, /device:TPU:0, one launch (start us, length us, event | category | flops | bytes accessed | tf_op | source)
XLA Modules:
  0.0 368.2 jit_solution(18147958280688204084)
XLA Ops:
  13.6 16.6 %all_gather.44 = f32[1536,4]{0,1:T(4,128)} all-gather(f32[384,4]{0,1:T(4,128)} %param.27), channel_id=1, replica_groups=mesh['grp'=2,'sp'=4,'tp'=4] {'sp'}, dimensions={0}, use_global_device_ids=true | all-gather | bytes 30720 | tf_op jit(solution)/shard_map/all_gather | solution.py:76
  30.3 18.2 %all_gather.39 = bf16[2048,128]{1,0:T(8,128)(2,1)} all-gather(bf16[512,128]{1,0:T(8,128)(2,1)S(1)} %copy-done.13), channel_id=1, replica_groups=mesh['grp'=2,'sp'=4,'tp'=4] {'sp'}, dimensions={0}, use_global_device_ids=true | all-gather | bytes 655360 | tf_op jit(solution)/shard_map/all_gather | solution.py:180
  49.2 22.0 %all_gather.38 = bf16[2048,128]{1,0:T(8,128)(2,1)} all-gather(bf16[512,128]{1,0:T(8,128)(2,1)S(1)} %copy-done.14), channel_id=1, replica_groups=mesh['grp'=2,'sp'=4,'tp'=4] {'sp'}, dimensions={0}, use_global_device_ids=true | all-gather | bytes 655360 | tf_op jit(solution)/shard_map/all_gather | solution.py:181
  77.0 25.7 %all_gather.42 = bf16[1536,4,64]{0,2,1:T(8,128)(2,1)S(1)} all-gather(bf16[384,4,64]{0,2,1:T(8,128)(2,1)S(1)} %multiply_convert_fusion.2), channel_id=1, replica_groups=mesh['grp'=2,'sp'=4,'tp'=4] {'sp'}, dimensions={0}, use_global_device_ids=true | all-gather | bytes 983040 | tf_op jit(solution)/shard_map/all_gather | solution.py:115
  102.7 5.0 %all-gather.17.cloned.1.call-done = bf16[2048,256]{1,0:T(8,128)(2,1)} async-done(((bf16[512,256]{1,0:T(8,128)(2,1)}), bf16[2048,256]{1,0:T(8,128)(2,1)}) %all-gather.17.cloned.1.call-update) | async-done | bytes 1048592 | tf_op jit(solution)/shard_map/all_gather | solution.py:184
  110.6 25.7 %all-gather.13.cloned.1.call-done = bf16[2048,256]{1,0:T(8,128)(2,1)} async-done(((bf16[512,256]{1,0:T(8,128)(2,1)}), bf16[2048,256]{1,0:T(8,128)(2,1)}) %all-gather.13.cloned.1.call-update) | async-done | bytes 1048592 | tf_op jit(solution)/shard_map/all_gather | solution.py:179
  145.1 4.0 %collective-permute-start.1 = (bf16[128,2,64]{0,2,1:T(8,128)(2,1)}, bf16[128,2,64]{0,2,1:T(8,128)(2,1)}, u32[]{:S(2)}, u32[]{:S(2)}) collective-permute-start(bf16[128,2,64]{0,2,1:T(8,128)(2,1)} %slice.68), channel_id=1, source_target_pairs={{0,4},{4,8},{8,12},{1,5},{5,9},{9,13},{2,6},{6,10},{10,14},{3,7},{... | collective-permute-start | bytes 98312 | tf_op jit(solution)/shard_map/ppermute | solution.py:16
  151.3 2.8 collective-permute-start
  156.6 8.5 %all-gather.19.cloned.1.call-done = bf16[2048,256]{1,0:T(8,128)(2,1)} async-done(((bf16[512,256]{1,0:T(8,128)(2,1)}), bf16[2048,256]{1,0:T(8,128)(2,1)}) %all-gather.19.cloned.1.call-update) | async-done | bytes 1048592 | tf_op jit(solution)/shard_map/all_gather | solution.py:182
  176.8 11.7 %collective-permute-done.3 = bf16[384,4,64]{0,2,1:T(8,128)(2,1)S(1)} collective-permute-done((bf16[384,4,64]{0,2,1:T(8,128)(2,1)}, bf16[384,4,64]{0,2,1:T(8,128)(2,1)S(1)}, u32[]{:S(2)}, u32[]{:S(2)}) %collective-permute-start.3) | collective-permute-done | bytes 196640 | tf_op jit(solution)/shard_map/ppermute | solution.py:118
  192.1 12.6 %collective-permute-done.4 = bf16[384,4,64]{0,2,1:T(8,128)(2,1)S(1)} collective-permute-done((bf16[384,4,64]{0,2,1:T(8,128)(2,1)S(1)}, bf16[384,4,64]{0,2,1:T(8,128)(2,1)S(1)}, u32[]{:S(2)}, u32[]{:S(2)}) %collective-permute-start.4) | collective-permute-done | bytes 196640 | tf_op jit(solution)/shard_map/ppermute | solution.py:118
  207.0 35.9 %conditional.1 = (f32[4,384]{1,0:T(4,128)}, f32[384,4,64]{0,2,1:T(8,128)}) conditional(s32[]{:T(128)} %bitcast.13, () %tuple.29, (bf16[1536,4,64]{0,2,1:T(8,128)(2,1)S(1)}, s32[]{:T(128)}, bf16[3072,4,64]{0,2,1:T(8,128)(2,1)S(1)}, f32[1536,4]{0,1:T(4,128)}, s32[3,512]{1,0:T(4,128)S(1)}, /*index=5*/s32[3,512]{1,0:T(4,128)S(1)}, s32[384]{0:T(512)}, ...), branch_computations={%region_7.8_spmd, %region_8.13_spmd} | conditional | flops 215199760 | bytes 16633765 | solution.py:143
  209.4 33.4 %while.26 = (s32[]{:T(128)}, f32[4,384]{1,0:T(4,128)S(1)}, f32[4,384]{1,0:T(4,128)}, f32[384,4,64]{0,2,1:T(8,128)}, s32[384]{0:T(512)}, /*index=5*/s32[3,512]{1,...) while((s32[]{:T(128)}, f32[4,384]{1,0:T(4,128)S(1)}, ...), condition=%wide.region_12.12_spmd.clone, body=%wide.region_9.11_spmd.clone.sunk | while | flops 215196672 | bytes 11896481 | solution.py:138
  211.7 2.7 fusion.85
  217.3 2.7 fusion.89
  222.3 2.7 fusion.85
  228.6 2.9 fusion.89
  233.7 2.7 fusion.85
  240.0 2.9 fusion.89
  246.3 22.5 %all-gather.21.cloned.1.call-done = bf16[384,2,1024]{2,0,1:T(8,128)(2,1)} async-done(((bf16[384,2,256]{2,0,1:T(8,128)(2,1)}), bf16[384,2,1024]{2,0,1:T(8,128)(2,1)}) %all-gather.21.cloned.1.call-update) | async-done | bytes 1572880 | tf_op jit(solution)/shard_map/all_gather | solution.py:219
  268.8 3.0 convolution_bitcast_fusion
  271.9 79.3 %all-gather.11.cloned.1.call-done = bf16[2048,1024]{1,0:T(8,128)(2,1)} async-done(((bf16[512,1024]{1,0:T(8,128)(2,1)}), bf16[2048,1024]{1,0:T(8,128)(2,1)}) %all-gather.11.cloned.1.call-update) | async-done | bytes 4194320 | tf_op jit(solution)/shard_map/all_gather | solution.py:185
  351.2 5.3 %add_divide_fusion = f32[384,1024]{1,0:T(8,128)} fusion(bf16[384,2048]{1,0:T(8,128)(2,1)S(1)} %copy-done.1, bf16[2048,1024]{1,0:T(8,128)(2,1)} %all-gather.11.cloned.1.call-done), kind=kOutput, calls=%fused_computation.45 | convolution fusion | flops 1611792384 | bytes 7340032 | tf_op jit(solution)/shard_map/dot_general | solution.py:188
  356.5 2.6 reshape.264
  (165 shorter events, 71.3 us)
Async XLA Ops:
  6.5 23.8 %copy-start.13 = (bf16[512,128]{1,0:T(8,128)(2,1)S(1)}, bf16[512,128]{1,0:T(8,128)(2,1)}, u32[]{:S(2)}) copy-start(bf16[512,128]{1,0:T(8,128)(2,1)} %param.21) | copy-start | bytes 393220
  6.5 42.0 %copy-start.20 = (f32[4]{0:T(128)S(1)}, f32[4]{0:T(128)}, u32[]{:S(2)}) copy-start(f32[4]{0:T(128)} %param.23) | copy-start | bytes 52
  6.5 42.6 %copy-start.14 = (bf16[512,128]{1,0:T(8,128)(2,1)S(1)}, bf16[512,128]{1,0:T(8,128)(2,1)}, u32[]{:S(2)}) copy-start(bf16[512,128]{1,0:T(8,128)(2,1)} %param.22) | copy-start | bytes 393220
  6.5 65.4 %all-gather.9.cloned.1.call-start = ((), (), s32[]{:S(2)}) async-start(), calls=%async_computation | async-start | bytes 1966080 | tf_op jit(solution)/shard_map/all_gather | solution.py:170
  7.3 67.0 %all-gather.15.cloned.1.call-start = ((), (), s32[]{:S(2)}) async-start(), calls=%async_computation.3 | async-start | bytes 1310720 | tf_op jit(solution)/shard_map/all_gather | solution.py:183
  8.0 99.7 %all-gather.17.cloned.1.call-start = ((), (), s32[]{:S(2)}) async-start(), calls=%async_computation.4 | async-start | bytes 1310720 | tf_op jit(solution)/shard_map/all_gather | solution.py:184
  8.8 127.5 %all-gather.13.cloned.1.call-start = ((), (), s32[]{:S(2)}) async-start(), calls=%async_computation.2 | async-start | bytes 1310720 | tf_op jit(solution)/shard_map/all_gather | solution.py:179
  9.3 155.8 %all-gather.19.cloned.1.call-start = ((), (), s32[]{:S(2)}) async-start(), calls=%async_computation.5 | async-start | bytes 1310720 | tf_op jit(solution)/shard_map/all_gather | solution.py:182
  9.9 236.4 %all-gather.23.cloned.1.call-start = ((), (), s32[]{:S(2)}) async-start(), calls=%async_computation.7 | async-start | bytes 2621440 | tf_op jit(solution)/shard_map/all_gather | solution.py:214
  10.5 63.3 %copy-start.15 = (f32[2048]{0:T(1024)S(1)}, f32[2048]{0:T(1024)}, u32[]{:S(2)}) copy-start(f32[2048]{0:T(1024)} %param.18) | copy-start | bytes 24580
  10.5 258.3 %all-gather.21.cloned.1.call-start = ((), (), s32[]{:S(2)}) async-start(), calls=%async_computation.6 | async-start | bytes 1966080 | tf_op jit(solution)/shard_map/all_gather | solution.py:219
  74.3 90.8 %copy-start = (bf16[384,2048]{1,0:T(8,128)(2,1)}, bf16[384,2048]{1,0:T(8,128)(2,1)S(1)}, u32[]{:S(2)}) copy-start(bf16[384,2048]{1,0:T(8,128)(2,1)S(1)} %fusion.27) | copy-start | bytes 4718596
  109.7 65.6 %collective-permute-start.2 = (bf16[384,4,64]{0,2,1:T(8,128)(2,1)S(1)}, bf16[384,4,64]{0,2,1:T(8,128)(2,1)}, u32[]{:S(2)}, u32[]{:S(2)}) collective-permute-start(bf16[384,4,64]{0,2,1:T(8,128)(2,1)S(1)} %bitcast.162), channel_id=1, source_target_pairs={{0,4},{4,8},{8,12},{12,0},{1,5},{5,9},{9,13},{13,1},{2,6},{6,10},{... | collective-permute-start | bytes 589832 | tf_op jit(solution)/shard_map/ppermute | solution.py:118
  145.1 23.7 %collective-permute-start.1 = (bf16[128,2,64]{0,2,1:T(8,128)(2,1)}, bf16[128,2,64]{0,2,1:T(8,128)(2,1)}, u32[]{:S(2)}, u32[]{:S(2)}) collective-permute-start(bf16[128,2,64]{0,2,1:T(8,128)(2,1)} %slice.68), channel_id=1, source_target_pairs={{0,4},{4,8},{8,12},{1,5},{5,9},{9,13},{2,6},{6,10},{10,14},{3,7},{... | collective-permute-start | bytes 98312 | tf_op jit(solution)/shard_map/ppermute | solution.py:16
  151.3 19.6 %collective-permute-start = (bf16[128,2,64]{0,2,1:T(8,128)(2,1)}, bf16[128,2,64]{0,2,1:T(8,128)(2,1)}, u32[]{:S(2)}, u32[]{:S(2)}) collective-permute-start(bf16[128,2,64]{0,2,1:T(8,128)(2,1)} %bitcast.1), channel_id=1, source_target_pairs={{0,4},{4,8},{8,12},{1,5},{5,9},{9,13},{2,6},{6,10},{10,14},{3,7},{... | collective-permute-start | bytes 98312 | tf_op jit(solution)/shard_map/ppermute | solution.py:16
  156.6 10.5 %copy-start.19 = (f32[64]{0:T(128)S(1)}, f32[64]{0:T(128)}, u32[]{:S(2)}) copy-start(f32[64]{0:T(128)} %get-tuple-element.294) | copy-start | bytes 772
  156.6 12.2 %copy-start.8 = (bf16[384,2,64]{0,2,1:T(8,128)(2,1)S(1)}, bf16[384,2,64]{0,2,1:T(8,128)(2,1)}, u32[]{:S(2)}) copy-start(bf16[384,2,64]{0,2,1:T(8,128)(2,1)} %copy-done.7) | copy-start | bytes 294916
  174.6 15.3 %copy-start.11 = (bf16[6,64,2,64]{1,3,2,0:T(8,128)(2,1)S(1)}, bf16[6,64,2,64]{1,3,2,0:T(8,128)(2,1)}, u32[]{:S(2)}) copy-start(bf16[6,64,2,64]{1,3,2,0:T(8,128)(2,1)} %copy.34) | copy-start | bytes 294916
  174.6 15.3 %copy-start.12 = (bf16[6,64,2,64]{1,3,2,0:T(8,128)(2,1)S(1)}, bf16[6,64,2,64]{1,3,2,0:T(8,128)(2,1)}, u32[]{:S(2)}) copy-start(bf16[6,64,2,64]{1,3,2,0:T(8,128)(2,1)} %copy.33) | copy-start | bytes 294916
  175.3 13.2 %collective-permute-start.3 = (bf16[384,4,64]{0,2,1:T(8,128)(2,1)}, bf16[384,4,64]{0,2,1:T(8,128)(2,1)S(1)}, u32[]{:S(2)}, u32[]{:S(2)}) collective-permute-start(bf16[384,4,64]{0,2,1:T(8,128)(2,1)} %collective-permute-done.2), channel_id=1, source_target_pairs={{0,4},{4,8},{8,12},{12,0},{1,5},{5,9},{9,13},{13,1},{2,6},{6,10},{... | collective-permute-start | bytes 589832 | tf_op jit(solution)/shard_map/ppermute | solution.py:118
  188.5 16.2 %collective-permute-start.4 = (bf16[384,4,64]{0,2,1:T(8,128)(2,1)S(1)}, bf16[384,4,64]{0,2,1:T(8,128)(2,1)S(1)}, u32[]{:S(2)}, u32[]{:S(2)}) collective-permute-start(bf16[384,4,64]{0,2,1:T(8,128)(2,1)S(1)} %collective-permute-done.3), channel_id=1, source_target_pairs={{0,4},{4,8},{8,12},{12,0},{1,5},{5,9},{9,13},{13,1},{2,6},{6,10},{... | collective-permute-start | bytes 589832 | tf_op jit(solution)/shard_map/ppermute | solution.py:118
  207.0 37.2 %copy-start.6 = (bf16[384,1,256]{2,0,1:T(8,128)(2,1)S(1)}, bf16[384,1,256]{2,0,1:T(8,128)(2,1)}, u32[]{:S(2)}) copy-start(bf16[384,1,256]{2,0,1:T(8,128)(2,1)} %convert_element_type.84) | copy-start | bytes 589828
  244.9 106.2 %all-gather.11.cloned.1.call-start = ((), (), s32[]{:S(2)}) async-start(), calls=%async_computation.1 | async-start | bytes 5242880 | tf_op jit(solution)/shard_map/all_gather | solution.py:185
  246.3 104.9 %copy-start.1 = (bf16[384,2048]{1,0:T(8,128)(2,1)S(1)}, bf16[384,2048]{1,0:T(8,128)(2,1)}, u32[]{:S(2)}) copy-start(bf16[384,2048]{1,0:T(8,128)(2,1)} %copy-done) | copy-start | bytes 4718596
  (10 other events, 49.5 us)
Sparse Core Ops, SparseCore 0:
  8.9 22.3 all-gather.8
  32.9 37.8 all-gather.14
  72.3 35.3 all-gather.16
  109.1 27.1 all-gather.12
  137.7 27.3 all-gather.18
  166.5 55.1 all-gather.22
  245.1 23.7 all-gather.20
  270.4 80.7 all-gather.10
